TPU v7x, 32 devices: a whole 2x2x4 slice. The times are simulated.
32 devices in a mesh: sp: 16 (over z, x, core), tp: 2 (over y).
Axes of the slice: x: 2, y: 2, z: 4, core: 2. Of those that a mesh axis runs over, the one named last changes fastest.
Arguments:
- skip_connection_stream: bfloat16 [12288, 2048], P('sp'), may hold values from -6 to 6
- probing_vectors: bfloat16 [12288, 512], P('sp', 'tp'), may hold values from -6 to 6
- addressing_vectors: bfloat16 [12288, 512], P('sp', 'tp'), may hold values from -6 to 6
- mapped_payloads: bfloat16 [12288, 1024], P('sp', 'tp'), may hold values from -6 to 6
- emission_switch: bfloat16 [12288, 1024], P('sp', 'tp'), may hold values from -6 to 6
- lapse_preactivation: bfloat16 [12288, 512], P('sp', 'tp')
- lapse_shift_entries: float32 [512], P('tp')
- surplus_attenuation_terms: float32 [12288], P('sp'), may hold values from -0.7 to 0
- passage_label_per_token: int32 [12288], P('sp'), may hold values from 0 to 3, never falling along the last dimension, each value on 1 to 6144 neighbouring positions
- attention_group_rescaler: float32 [128], replicated, may hold values from 0.1 to 1.9
- emission_projector: bfloat16 [1024, 2048], P('tp'), may hold values from -0.1875 to 0.1875
- perceptron_rescaler: float32 [2048], replicated, may hold values from 0.1 to 1.9
- switching_projector: bfloat16 [2048, 5632], P('sp', 'tp'), may hold values from -0.125 to 0.125
- widening_projector: bfloat16 [2048, 5632], P('sp', 'tp'), may hold values from -0.125 to 0.125
- shrinking_projector: bfloat16 [5632, 2048], P('tp', 'sp'), may hold values from -0.078125 to 0.078125
Outputs:
- layer_out: bfloat16 [12288, 2048], P(('sp', 'tp'))
Inputs may be any that keep to these rules, and one draw needn't show every extreme that they name: `passage_label_per_token`: document numbers never fall along the sequence; a document holds at most 6144 positions.
All inputs are finite; a program needn't handle non-finite values.
Results may differ from a plain program's by a relative error of at most 0.014.
Values may be sent and summed in bfloat16 or wider, within the bound.
No kernel may reach another device: no remote copies, remote signals or barrier semaphores. Data moves between devices by JAX's collectives and lax.ppermute only.
A program may use at most 128 MiB of HBM per device.

v0:
```python
import jax
import jax.numpy as jnp
from jax import lax
from jax.sharding import PartitionSpec as P

DK = 64
DV = 128
BLOCK = 64


eps = 1e-06
sharpness_factor = 16.0


def entering(shard, axis, join, neutral):
    place = lax.axis_index(axis)
    gathered = jax.tree.map(
        lambda a, kind: lax.all_gather(a.astype(kind), axis),
        shard,
        jax.tree.map(lambda a: jnp.bfloat16 if a.dtype == jnp.float32 else a.dtype, shard),
    )
    state = jax.tree.map(lambda a, e: jnp.zeros_like(a) + jnp.asarray(e, a.dtype), shard, neutral)

    def one(turn, state):
        return join(
            state,
            jax.tree.map(
                lambda a, own: lax.dynamic_index_in_dim(a, turn, 0, False).astype(own.dtype),
                gathered,
                shard,
            ),
        )

    return lax.fori_loop(0, place, one, state)


def head_split(array, heads):
    return array.reshape(array.shape[0], heads, -1).transpose(1, 0, 2)


def block_pass(
    query_head_rows,
    key_heads,
    value_heads,
    decay_heads,
    documents,
    recurrent_state,
    last_doc,
    offset,
    span,
):
    heads, length, _ = query_head_rows.shape
    blocks = length // span
    middle = span // 2

    def to_blocks(array):
        return array.reshape(heads, blocks, span, array.shape[-1]).transpose(1, 0, 2, 3)

    lower = jnp.tril(jnp.ones((span, span), dtype=bool))

    def step(carry, inputs):
        recurrent_state, last_doc, offset = carry
        query_block, key_blk, value_block, piece_attenuation, doc_blk = inputs
        cumulative_decay = jnp.cumsum(piece_attenuation, axis=1)
        previous_valid = (doc_blk == last_doc).astype(jnp.float32)
        cross_block_output = (
            jnp.einsum("gfl,glm->gfm", query_block * jnp.exp(cumulative_decay), recurrent_state)
            * previous_valid[None, :, None]
        )
        centre = cumulative_decay[:, middle : middle + 1, :]
        query_scaled = query_block * jnp.exp(cumulative_decay - centre)
        key_scaled = key_blk * jnp.exp(centre - cumulative_decay)
        same = (doc_blk[:, None] == doc_blk[None, :]) & lower
        raw_scores = jnp.einsum("hik,hjk->hij", query_scaled, key_scaled)
        scores = jnp.where(same[None, :, :], raw_scores, 0.0)
        result = cross_block_output + jnp.einsum("hij,hjv->hiv", scores, value_block)
        final_memory_summary = cumulative_decay[:, -1, :]
        last_valid = (doc_blk[-1] == last_doc).astype(jnp.float32)
        tail_ok = (doc_blk == doc_blk[-1]).astype(jnp.float32)
        decayed_keys = (
            key_blk
            * jnp.exp(final_memory_summary[:, None, :] - cumulative_decay)
            * tail_ok[None, :, None]
        )
        recurrent_state = recurrent_state * jnp.exp(final_memory_summary)[
            :, :, None
        ] * last_valid + jnp.einsum("wrz,wrs->wzs", decayed_keys, value_block)
        return (
            (recurrent_state, doc_blk[-1], offset + final_memory_summary),
            (result, cumulative_decay + offset[:, None, :]),
        )

    carry, outputs = lax.scan(
        step,
        (recurrent_state, last_doc, offset),
        (
            to_blocks(query_head_rows),
            to_blocks(key_heads),
            to_blocks(value_heads),
            to_blocks(decay_heads),
            documents.reshape(blocks, span),
        ),
    )
    result, running_state = outputs
    result = result.transpose(1, 0, 2, 3).reshape(heads, length, -1)
    running_state = running_state.transpose(1, 0, 2, 3).reshape(heads, length, -1)
    return (carry[0], carry[2], result, running_state)


def join_spans(earlier, later):
    linked = ((earlier[3] == later[2]) | (earlier[3] < 0.0) | (later[2] < 0.0)).astype(jnp.float32)
    decay_total = earlier[0] * later[0] * linked
    state_total = earlier[1] * (later[0] * linked)[:, :, None] + later[1]
    first_doc = jnp.where(earlier[2] < 0.0, later[2], earlier[2])
    final_doc = jnp.where(later[3] < 0.0, earlier[3], later[3])
    return (decay_total, state_total, first_doc, final_doc)


def rms_rows(rows, gain):
    wide = rows.astype(jnp.float32)
    return (wide * lax.rsqrt(jnp.mean(wide * wide, axis=-1, keepdims=True) + eps) * gain).astype(
        jnp.bfloat16
    )


def per_device(
    skip_connection_stream,
    probing_vectors,
    addressing_vectors,
    mapped_payloads,
    emission_switch,
    lapse_preactivation,
    lapse_shift_entries,
    surplus_attenuation_terms,
    passage_label_per_token,
    attention_group_rescaler,
    emission_projector,
    perceptron_rescaler,
    switching_projector,
    widening_projector,
    shrinking_projector,
):
    rows_here = skip_connection_stream.shape[0]
    heads_here = probing_vectors.shape[1] // DK
    keeping_exponent = (
        jax.nn.log_sigmoid(lapse_preactivation.astype(jnp.float32) + lapse_shift_entries[None, :])
        / sharpness_factor
        + surplus_attenuation_terms[:, None]
    )
    query_head_rows = head_split(probing_vectors.astype(jnp.float32) * DK ** (-0.5), heads_here)
    key_heads = head_split(addressing_vectors.astype(jnp.float32), heads_here)
    value_heads = head_split(mapped_payloads.astype(jnp.float32), heads_here)
    decay_heads = head_split(keeping_exponent, heads_here)
    zero_state = jnp.zeros((heads_here, DK, DV), jnp.float32)
    state_local, total_log, local_out, running_state = block_pass(
        query_head_rows,
        key_heads,
        value_heads,
        decay_heads,
        passage_label_per_token,
        zero_state,
        passage_label_per_token[0],
        jnp.zeros((heads_here, DK), jnp.float32),
        BLOCK,
    )
    unbroken = (passage_label_per_token[0] == passage_label_per_token[-1]).astype(jnp.float32)
    summary = (
        jnp.exp(total_log) * unbroken,
        state_local,
        passage_label_per_token[0].astype(jnp.float32),
        passage_label_per_token[-1].astype(jnp.float32),
    )
    identity = (
        jnp.ones_like(total_log),
        jnp.zeros_like(state_local),
        jnp.full((), -1.0, jnp.float32),
        jnp.full((), -1.0, jnp.float32),
    )
    carried_state = entering(summary, "sp", join_spans, identity)
    reaches = (passage_label_per_token.astype(jnp.float32) == carried_state[3]).astype(jnp.float32)
    incoming = (
        jnp.einsum("qlj,qjf->qlf", query_head_rows * jnp.exp(running_state), carried_state[1])
        * reaches[None, :, None]
    )
    attn = local_out + incoming
    normed_attn = (
        attn
        * lax.rsqrt(jnp.mean(attn * attn, axis=-1, keepdims=True) + eps)
        * attention_group_rescaler
    )
    flat = normed_attn.transpose(1, 0, 2).reshape(rows_here, heads_here * DV)
    gated = (flat * jax.nn.silu(emission_switch.astype(jnp.float32))).astype(jnp.bfloat16)
    share_rows = rows_here // lax.axis_size("tp")
    own_start = lax.axis_index("tp") * share_rows
    mixed = lax.psum(
        jnp.dot(gated, emission_projector, preferred_element_type=jnp.float32).astype(jnp.bfloat16),
        "tp",
    ).astype(jnp.float32)
    first_all = (skip_connection_stream.astype(jnp.float32) + mixed).astype(jnp.bfloat16)
    normed = rms_rows(first_all, perceptron_rescaler)
    first_own = lax.dynamic_slice_in_dim(first_all, own_start, share_rows, 0)
    gate = jnp.dot(
        normed,
        lax.all_gather(switching_projector, "sp", axis=0, tiled=True),
        preferred_element_type=jnp.float32,
    )
    upper = jnp.dot(
        normed,
        lax.all_gather(widening_projector, "sp", axis=0, tiled=True),
        preferred_element_type=jnp.float32,
    )
    hidden = (jax.nn.silu(gate) * upper).astype(jnp.bfloat16)
    terms = jnp.dot(
        hidden,
        lax.all_gather(shrinking_projector, "sp", axis=1, tiled=True),
        preferred_element_type=jnp.float32,
    )
    ffn_out = lax.psum_scatter(
        terms.astype(jnp.bfloat16), "tp", scatter_dimension=0, tiled=True
    ).astype(jnp.float32)
    return (first_own.astype(jnp.float32) + 0.5 * ffn_out).astype(jnp.bfloat16)


def solution(mesh):
    placed = (
        P("sp", None),
        P("sp", "tp"),
        P("sp", "tp"),
        P("sp", "tp"),
        P("sp", "tp"),
        P("sp", "tp"),
        P("tp"),
        P("sp"),
        P("sp"),
        P(),
        P("tp", None),
        P(),
        P("sp", "tp"),
        P("sp", "tp"),
        P("tp", "sp"),
    )
    return jax.shard_map(
        per_device, mesh=mesh, in_specs=placed, out_specs=P(("sp", "tp"), None), check_vma=False
    )
```

profile of v0, /device:TPU:0, one launch (start us, length us, event | category | flops | bytes accessed | tf_op | source)
XLA Modules:
  0.0 747.7 jit_solution(6886762841094768849)
XLA Ops:
  10.6 1.8 reshape.144
  14.6 2.7 reshape.150
  19.1 1.8 reshape.137
  23.6 117.2 %while.35 = (s32[]{:T(128)}, f32[4,64,128]{2,1,0:T(8,128)S(1)}, s32[]{:T(128)}, f32[4,64]{1,0:T(4,128)S(1)}, f32[12,4,64,128]{3,2,0,1:T(8,128)}, /*index=5*/f32[...) while((s32[]{:T(128)}, f32[4,64,128]{2,1,0:T(8,128)S(1)}, ...), condition=%wide.region_2.3_spmd.clone, body=%wide.region_0.2_spmd.clone.sunk | while | flops 16118533 | bytes 2851019 | solution.py:93
  27.4 1.8 fusion.85
  37.2 1.8 fusion.85
  46.9 1.8 fusion.85
  56.7 1.8 fusion.85
  66.5 1.8 fusion.85
  76.2 1.8 fusion.85
  95.8 1.8 fusion.85
  105.5 1.8 fusion.85
  125.1 1.8 fusion.85
  134.8 1.8 fusion.85
  144.9 35.1 %all-reduce.2 = (bf16[16]{0:T(256)(128)(2,1)S(1)}, bf16[16]{0:T(256)(128)(2,1)S(1)}) all-reduce(bf16[16]{0:T(256)(128)(2,1)S(1)} %dynamic-update-slice, bf16[16]{0:T(256)(128)(2,1)S(1)} %dynamic-update-slice.1), channel_id=1, replica_groups=mesh['sp'=16,'tp'=2] {'sp'}, use_global_device_ids=true, to_apply=%add | all-reduce | flops 32 | bytes 128
  181.2 2.8 exponential_bitcast_fusion
  184.0 3.0 copy.57
  186.9 2.7 exp.47
  189.6 3.1 copy.58
  192.8 17.1 %all-gather.2 = bf16[16,4,64]{2,1,0:T(4,128)(2,1)S(1)} all-gather(bf16[1,4,64]{2,1,0:T(4,128)(2,1)S(1)} %fusion.58), channel_id=2, replica_groups=mesh['sp'=16,'tp'=2] {'sp'}, dimensions={0}, use_global_device_ids=true | all-gather | bytes 8704 | tf_op jit(solution)/shard_map/all_gather | solution.py:18
  210.0 2.1 multiply_reduce_fusion
  213.5 3.0 copy.59
  216.6 4.9 convolution_convert_fusion
  223.6 154.7 %all-reduce.5.cloned.1.call-done = bf16[768,2048]{1,0:T(8,128)(2,1)} async-done(((bf16[768,2048]{1,0:T(8,128)(2,1)}), bf16[768,2048]{1,0:T(8,128)(2,1)}) %all-reduce.5.cloned.1.call-update) | async-done | bytes 3145744 | tf_op jit(solution)/shard_map/psum | solution.py:195
  378.3 6.0 fusion.36
  384.3 90.3 %all-gather.8.cloned.1.call-done = bf16[2048,2816]{1,0:T(8,128)(2,1)} async-done(((bf16[128,2816]{1,0:T(8,128)(2,1)}), bf16[2048,2816]{1,0:T(8,128)(2,1)}) %all-gather.8.cloned.1.call-update) | async-done | bytes 11534352 | tf_op jit(solution)/shard_map/all_gather | solution.py:204
  474.6 15.9 %fusion.49 = f32[768,2816]{1,0:T(8,128)} fusion(bf16[2048,2816]{1,0:T(8,128)(2,1)} %all-gather.8.cloned.1.call-done, bf16[768,2048]{1,0:T(8,128)(2,1)} %get-tuple-element.262, f32[2048]{0:T(1024)S(1)} %copy-done.9, f32[768]{0:T(1024)S(1)} %add_rsqrt_fusion.1), kind=kOutput, calls=%fused_computation.73 | convolution fusion | flops 8864661504 | bytes 23342080 | tf_op jit(solution)/shard_map/dot_general | solution.py:202
  490.6 78.5 %all-gather.10.cloned.1.call-done = bf16[2048,2816]{1,0:T(8,128)(2,1)} async-done(((bf16[128,2816]{1,0:T(8,128)(2,1)}), bf16[2048,2816]{1,0:T(8,128)(2,1)}) %all-gather.10.cloned.1.call-update) | async-done | bytes 11534352 | tf_op jit(solution)/shard_map/all_gather | solution.py:209
  569.0 97.2 %all-gather.12.cloned.1.call-done = bf16[2816,2048]{1,0:T(8,128)(2,1)} async-done(((bf16[2816,128]{1,0:T(8,128)(2,1)}), bf16[2816,2048]{1,0:T(8,128)(2,1)}) %all-gather.12.cloned.1.call-update) | async-done | bytes 11534352 | tf_op jit(solution)/shard_map/all_gather | solution.py:215
  666.2 29.2 %fusion.41 = bf16[768,2048]{1,0:T(8,128)(2,1)} fusion(bf16[2816,2048]{1,0:T(8,128)(2,1)} %all-gather.12.cloned.1.call-done, f32[768,2816]{1,0:T(8,128)} %fusion.49, bf16[2048,2816]{1,0:T(8,128)(2,1)} %all-gather.10.cloned.1.call-done, bf16[768,2048]{1,0:T(8,128)(2,1)} %get-tuple-element.262, f32[2048]{0:T(1024)S(1)} %copy-done.9, f32[768]{0:T(1024)S(1)} %add_rsqrt_fusion.1), kind=kOutput, calls=%fused_computation.57 | convolution fusion | flops 17737580544 | bytes 38022144 | tf_op jit(solution)/shard_map/dot_general | solution.py:213
  695.4 41.7 %reduce-scatter.2.cloned.1.call-done = bf16[384,2048]{1,0:T(8,128)(2,1)} async-done(((bf16[768,2048]{1,0:T(8,128)(2,1)}), bf16[384,2048]{1,0:T(8,128)(2,1)}) %reduce-scatter.2.cloned.1.call-update) | async-done | bytes 1572880 | tf_op jit(solution)/shard_map/reduce_scatter | solution.py:218
  737.1 3.7 add_convert_fusion.1
  (244 shorter events, 100.5 us)
Async XLA Ops:
  6.5 210.0 %copy-start = (bf16[512,2048]{1,0:T(8,128)(2,1)S(1)}, bf16[512,2048]{1,0:T(8,128)(2,1)}, u32[]{:S(2)}) copy-start(bf16[512,2048]{1,0:T(8,128)(2,1)} %param.29) | copy-start | bytes 6291460
  6.5 203.4 %all-gather.14.cloned.1.call-start = ((), (), s32[]{:S(2)}) async-start(), calls=%async_computation.6 | async-start | bytes 1114112 | tf_op jit(solution)/shard_map/all_gather | solution.py:18
  10.6 6.7 copy-start.2
  12.4 6.1 copy-start.5
  12.5 6.1 copy-start.6
  23.6 119.2 %copy-start.10 = (u32[32]{0:T(128)S(1)}, u32[32]{0:T(128)}, u32[]{:S(2)}) copy-start(u32[32]{0:T(128)} %constant.98) | copy-start | bytes 388
  141.5 236.9 %all-reduce.5.cloned.1.call-start = ((), (), s32[]{:S(2)}) async-start(), calls=%async_computation.1 | async-start | bytes 6291456 | tf_op jit(solution)/shard_map/psum | solution.py:195
  189.6 20.3 %copy-start.4 = (s32[768]{0:T(1024)S(1)}, s32[768]{0:T(1024)}, u32[]{:S(2)}) copy-start(s32[768]{0:T(1024)} %param.27) | copy-start | bytes 9220
  189.6 20.4 %copy-start.3 = (f32[768,256]{0,1:T(8,128)S(1)}, f32[768,256]{0,1:T(8,128)}, u32[]{:S(2)}) copy-start(f32[768,256]{0,1:T(8,128)} %copy-done.2) | copy-start | bytes 2359300
  209.9 2.2 copy-start.7
  212.2 4.4 copy-start.8
  221.5 253.2 %all-gather.8.cloned.1.call-start = ((), (), s32[]{:S(2)}) async-start(), calls=%async_computation.2 | async-start | bytes 12255232 | tf_op jit(solution)/shard_map/all_gather | solution.py:204
  222.2 346.8 %all-gather.10.cloned.1.call-start = ((), (), s32[]{:S(2)}) async-start(), calls=%async_computation.3 | async-start | bytes 12255232 | tf_op jit(solution)/shard_map/all_gather | solution.py:209
  222.8 443.4 %all-gather.12.cloned.1.call-start = ((), (), s32[]{:S(2)}) async-start(), calls=%async_computation.4 | async-start | bytes 12255232 | tf_op jit(solution)/shard_map/all_gather | solution.py:215
  223.4 251.3 %copy-start.9 = (f32[2048]{0:T(1024)S(1)}, f32[2048]{0:T(1024)}, u32[]{:S(2)}) copy-start(f32[2048]{0:T(1024)} %param.30) | copy-start | bytes 24580
  223.4 513.7 %reduce-scatter.2.cloned.1.call-start = ((), (), s32[]{:S(2)}) async-start(), calls=%async_computation.5 | async-start | bytes 4718592 | tf_op jit(solution)/shard_map/reduce_scatter | solution.py:218
  695.4 45.4 %copy-start.1 = (bf16[512,2048]{1,0:T(8,128)(2,1)S(1)}, bf16[512,2048]{1,0:T(8,128)(2,1)}, u32[]{:S(2)}) copy-start(bf16[512,2048]{1,0:T(8,128)(2,1)} %param.29) | copy-start | bytes 6291460
Sparse Core Ops, SparseCore 0:
  141.6 40.5 all-gather.13
  221.6 156.6 all-reduce.4
  380.6 93.9 all-gather.7
  476.8 92.2 all-gather.9
  571.0 95.1 all-gather.11
  695.5 41.5 reduce-scatter.1
where the time goes:
time: 752 us; the launch traced here: 748 us
  waiting for transfers between devices  464 us (62%)
  matrix products  89.2 us (12%)
  local copies, waits for them, and re-layouts  78.8 us (10%)
  blocking collectives  52.2 us (7%)
  other arithmetic  31.1 us (4%)
  between operations  16.8 us (2%)
  loops' own time  15 us (2%)
    psum x1, waiting for transfers between devices, per_device(): lax.psum(jnp.dot(gated, emission_projector, preferred_element_type=jnp.fl...  155 us
    all_gather x1, waiting for transfers between devices, per_device(): lax.all_gather(shrinking_projector, 'sp', axis=1, tiled=True)  97.2 us
    all_gather x1, waiting for transfers between devices, per_device(): lax.all_gather(switching_projector, 'sp', axis=0, tiled=True)  90.3 us
    all_gather x1, waiting for transfers between devices, per_device(): lax.all_gather(widening_projector, 'sp', axis=0, tiled=True)  78.5 us
    reduce_scatter x1, waiting for transfers between devices, per_device(): lax.psum_scatter(terms.astype(jnp.bfloat16), 'tp', scatter_dimension=0, t...  41.7 us
    dynamic_slice x60, local copies, waits for them, and re-layouts, block_pass(): lax.scan(step, (recurrent_state, last_doc, offset), (to_blocks(query_head...  40.2 us
    unnamed x1, blocking collectives  35.1 us
    dot_general x1, matrix products, per_device(): jnp.dot(hidden, lax.all_gather(shrinking_projector, 'sp', axis=1, tiled=T...  29.2 us
  transfers between devices with their start and end apart: 6, of which 5 were waited for; matrix products, arithmetic and copies ran while one was open for 5% of the time, Pallas kernels for 0%

commit v1 on v0

v1 whole, which is shorter than its diff:
```python
import jax
import jax.numpy as jnp
from jax import lax
from jax.experimental import pallas as pl
from jax.experimental.pallas import tpu as pltpu
from jax.sharding import PartitionSpec as P

DK = 64
DV = 128
BLOCK = 64

eps = 1e-06
sharpness_factor = 16.0

NN = (((1,), (0,)), ((), ()))
NT = (((1,), (1,)), ((), ()))
TN = (((0,), (0,)), ((), ()))


def mm(a, b, dims):
    return lax.dot_general(
        a.astype(jnp.bfloat16), b.astype(jnp.bfloat16), dims, preferred_element_type=jnp.float32
    )


def local_kernel(
    q_ref, k_ref, v_ref, f_ref, shift_ref, extra_ref, doc_ref, docrow_ref,
    out_ref, qrun_ref, state_ref, total_ref, ld_ref,
):
    rows, width = q_ref.shape
    pairs = width // (2 * DK)
    blocks = rows // BLOCK
    pre = f_ref[...].astype(jnp.float32) + shift_ref[...]
    ld_ref[...] = (
        jnp.minimum(pre, 0.0) - jnp.log1p(jnp.exp(-jnp.abs(pre)))
    ) / sharpness_factor + extra_ref[...]
    r = lax.broadcasted_iota(jnp.int32, (BLOCK, BLOCK), 0)
    c = lax.broadcasted_iota(jnp.int32, (BLOCK, BLOCK), 1)
    lower = c <= r
    tril = lower.astype(jnp.float32)
    half = lax.broadcasted_iota(jnp.int32, (BLOCK, 2 * DK), 1) < DK
    sr = lax.broadcasted_iota(jnp.int32, (2 * DK, 2 * DV), 0) < DK
    sc = lax.broadcasted_iota(jnp.int32, (2 * DK, 2 * DV), 1) < DV
    diag = sr == sc
    state = [jnp.zeros((2 * DK, 2 * DV), jnp.float32) for _ in range(pairs)]
    offset = jnp.zeros((1, width), jnp.float32)
    last = doc_ref[0:1, :]
    for b in range(blocks):
        at = slice(b * BLOCK, (b + 1) * BLOCK)
        cum = lax.dot_general(
            tril, ld_ref[at, :], NN, precision=lax.Precision.HIGHEST,
            preferred_element_type=jnp.float32,
        )
        doc = doc_ref[at, :]
        docrow = docrow_ref[b : b + 1, :]
        end = doc_ref[(b + 1) * BLOCK - 1 : (b + 1) * BLOCK, :]
        same = (doc == docrow) & lower
        prev_ok = (doc == last).astype(jnp.float32)
        tail_ok = (doc == end).astype(jnp.float32)
        last_ok = (end == last).astype(jnp.float32)
        q = q_ref[at, :].astype(jnp.float32) * DK ** (-0.5)
        k = k_ref[at, :].astype(jnp.float32)
        final = cum[BLOCK - 1 : BLOCK, :]
        centre = cum[BLOCK // 2 : BLOCK // 2 + 1, :]
        qe = q * jnp.exp(cum)
        qs = q * jnp.exp(cum - centre)
        ks = (k * jnp.exp(centre - cum)).astype(jnp.bfloat16)
        kd = k * jnp.exp(final - cum) * tail_ok
        qrun_ref[at, :] = (qe * jnp.exp(offset)).astype(jnp.bfloat16)
        fall = jnp.exp(final) * last_ok
        for p in range(pairs):
            kk = slice(p * 2 * DK, (p + 1) * 2 * DK)
            vv = slice(p * 2 * DV, (p + 1) * 2 * DV)
            v = v_ref[at, vv]
            cross = mm(qe[:, kk], state[p], NN) * prev_ok
            sa = mm(jnp.where(half, qs[:, kk], 0.0), ks[:, kk], NT)
            sb = mm(jnp.where(half, 0.0, qs[:, kk]), ks[:, kk], NT)
            oa = mm(jnp.where(same, sa, 0.0), v[:, :DV], NN)
            ob = mm(jnp.where(same, sb, 0.0), v[:, DV:], NN)
            out_ref[at, vv] = cross + jnp.concatenate([oa, ob], axis=1)
            fresh = mm(kd[:, kk], v, TN)
            decay = jnp.transpose(jnp.broadcast_to(fall[:, kk], (8, 2 * DK)))[:, 0:1]
            state[p] = state[p] * decay + jnp.where(diag, fresh, 0.0)
        offset = offset + final
        last = end
    for p in range(pairs):
        state_ref[(2 * p) * DK : (2 * p + 1) * DK, :] = state[p][:DK, :DV].astype(jnp.bfloat16)
        state_ref[(2 * p + 1) * DK : (2 * p + 2) * DK, :] = state[p][DK:, DV:].astype(jnp.bfloat16)
    total_ref[...] = offset


def finish_kernel(out_ref, qrun_ref, state_ref, reach_ref, gain_ref, gate_ref, gated_ref):
    heads = out_ref.shape[1] // DV
    reach = reach_ref[...]
    gain = gain_ref[...]
    for h in range(heads):
        p = h // 2
        q = qrun_ref[:, p * 2 * DK : (p + 1) * 2 * DK]
        s = state_ref[p * 2 * DK : (p + 1) * 2 * DK, :]
        keep = (lax.broadcasted_iota(jnp.int32, s.shape, 0) < DK) == (h % 2 == 0)
        s = jnp.where(keep, s, 0.0)
        vv = slice(h * DV, (h + 1) * DV)
        attn = out_ref[:, vv] + mm(q, s, NN) * reach
        mean = jnp.mean(attn * attn, axis=-1, keepdims=True)
        g = gate_ref[:, vv].astype(jnp.float32)
        gated_ref[:, vv] = (
            attn * lax.rsqrt(mean + eps) * gain * (g / (1.0 + jnp.exp(-g)))
        ).astype(jnp.bfloat16)


def rms_rows(rows, gain):
    wide = rows.astype(jnp.float32)
    return (wide * lax.rsqrt(jnp.mean(wide * wide, axis=-1, keepdims=True) + eps) * gain).astype(
        jnp.bfloat16
    )


def shift(a, axis, k):
    n = lax.axis_size(axis)
    return lax.ppermute(a, axis, [(i, (i + k) % n) for i in range(n)])


def carried(state, decay, first, final, heads):
    n = lax.axis_size("sp")
    place = lax.axis_index("sp")
    states = lax.all_gather(state, "sp")
    small = jnp.concatenate(
        [
            decay.reshape(heads, DK),
            jnp.full((1, DK), first, jnp.float32),
            jnp.full((1, DK), final, jnp.float32),
        ],
        axis=0,
    ).astype(jnp.bfloat16)
    smalls = lax.all_gather(small, "sp").astype(jnp.float32)
    decays = smalls[:, :heads].reshape(n, heads * DK)
    firsts = smalls[:, heads, 0]
    finals = smalls[:, heads + 1, 0]
    linked = jnp.concatenate([jnp.zeros((1,)), (finals[:-1] == firsts[1:]).astype(jnp.float32)])
    run = jnp.ones((heads * DK,), jnp.float32)
    total = jnp.zeros(state.shape, jnp.float32)
    for j in reversed(range(n)):
        before = j < place
        total = total + jnp.where(before, run, 0.0)[:, None] * states[j].astype(jnp.float32)
        run = jnp.where(before, run * decays[j] * linked[j], run)
    doc = jnp.where(place > 0, lax.dynamic_index_in_dim(finals, jnp.maximum(place - 1, 0), 0, False), -1.0)
    return total, doc


def per_device(
    skip_connection_stream,
    probing_vectors,
    addressing_vectors,
    mapped_payloads,
    emission_switch,
    lapse_preactivation,
    lapse_shift_entries,
    surplus_attenuation_terms,
    passage_label_per_token,
    attention_group_rescaler,
    emission_projector,
    perceptron_rescaler,
    switching_projector,
    widening_projector,
    shrinking_projector,
):
    rows, width = probing_vectors.shape
    heads = width // DK
    tp = lax.axis_size("tp")
    mine = lax.axis_index("tp")

    switching = lax.all_gather(switching_projector, "sp", axis=0, tiled=True)
    widening = lax.all_gather(widening_projector, "sp", axis=0, tiled=True)
    shrinking = lax.all_gather(shrinking_projector, "sp", axis=1, tiled=True)
    projectors = [emission_projector] + [shift(emission_projector, "tp", k) for k in range(1, tp)]

    docs = passage_label_per_token
    f32 = jnp.float32
    local_out, qrun, state, total = pl.pallas_call(
        local_kernel,
        out_shape=(
            jax.ShapeDtypeStruct((rows, heads * DV), f32),
            jax.ShapeDtypeStruct((rows, width), jnp.bfloat16),
            jax.ShapeDtypeStruct((heads * DK, DV), jnp.bfloat16),
            jax.ShapeDtypeStruct((1, width), f32),
        ),
        scratch_shapes=[pltpu.VMEM((rows, width), f32)],
        name="local_pass",
    )(
        probing_vectors,
        addressing_vectors,
        mapped_payloads,
        lapse_preactivation,
        lapse_shift_entries[None, :],
        surplus_attenuation_terms[:, None],
        docs[:, None],
        docs.reshape(rows // BLOCK, BLOCK),
    )
    first = docs[0].astype(f32)
    final = docs[-1].astype(f32)
    unbroken = (first == final).astype(f32)
    state_in, doc_in = carried(state, jnp.exp(total[0]) * unbroken, first, final, heads)
    reach = (docs.astype(f32) == doc_in).astype(f32)[:, None]
    gated = pl.pallas_call(
        finish_kernel,
        out_shape=jax.ShapeDtypeStruct((rows, heads * DV), jnp.bfloat16),
        name="finish_pass",
    )(local_out, qrun, state_in, reach, attention_group_rescaler[None, :], emission_switch)

    others = [gated] + [shift(gated, "tp", k) for k in range(1, tp)]
    mixed = jnp.zeros((rows, skip_connection_stream.shape[1]), f32)
    for g, w in zip(others, projectors):
        mixed = mixed + jnp.dot(g, w, preferred_element_type=f32)
    first_all = (skip_connection_stream.astype(f32) + mixed).astype(jnp.bfloat16)
    normed = rms_rows(first_all, perceptron_rescaler)
    gate = jnp.dot(normed, switching, preferred_element_type=f32)
    upper = jnp.dot(normed, widening, preferred_element_type=f32)
    hidden = (jax.nn.silu(gate) * upper).astype(jnp.bfloat16)

    share = rows // tp
    parts = 2
    step = share // parts
    arrived = []
    for k in range(1, tp):
        start = ((mine + k) % tp) * share
        for i in range(parts):
            sent = jnp.dot(
                lax.dynamic_slice_in_dim(hidden, start + i * step, step, 0),
                shrinking,
                preferred_element_type=f32,
            ).astype(jnp.bfloat16)
            arrived.append((i, shift(sent, "tp", k)))
    own = jnp.dot(
        lax.dynamic_slice_in_dim(hidden, mine * share, share, 0),
        shrinking,
        preferred_element_type=f32,
    )
    first_own = lax.dynamic_slice_in_dim(first_all, mine * share, share, 0).astype(f32)
    outs = []
    for i in range(parts):
        at = slice(i * step, (i + 1) * step)
        ffn = own[at].astype(jnp.bfloat16).astype(f32)
        for j, piece in arrived:
            if j == i:
                ffn = ffn + piece.astype(f32)
        outs.append((first_own[at] + 0.5 * ffn).astype(jnp.bfloat16))
    return jnp.concatenate(outs, axis=0)


def solution(mesh):
    placed = (
        P("sp", None),
        P("sp", "tp"),
        P("sp", "tp"),
        P("sp", "tp"),
        P("sp", "tp"),
        P("sp", "tp"),
        P("tp"),
        P("sp"),
        P("sp"),
        P(),
        P("tp", None),
        P(),
        P("sp", "tp"),
        P("sp", "tp"),
        P("tp", "sp"),
    )
    return jax.shard_map(
        per_device, mesh=mesh, in_specs=placed, out_specs=P(("sp", "tp"), None), check_vma=False
    )
```

time: 752 us -> 402 us (0.53)
  waiting for transfers between devices: 464 us -> 263 us
  local copies, waits for them, and re-layouts: 78.8 us -> 11.1 us
  matrix products: 89.2 us -> 54.1 us
  blocking collectives: 52.2 us -> 21.8 us
  other arithmetic: 31.1 us -> 15.1 us
  loops' own time: 15 us -> 0 us
  Pallas kernels: 0 us -> 13.9 us
    psum x1 -> x0, waiting for transfers between devices: 155 us -> none  [per_device(): lax.psum(jnp.dot(gated, emission_projector, preferred_element_type=jnp.fl...]
    all_gather x4, waiting for transfers between devices: 266 us -> 219 us  [the longest x1 80.1 us: per_device(): shrinking = lax.all_gather(shrinking_projector, 'sp', axis=1, tiled=True)]
    ppermute x0 -> x4, waiting for transfers between devices: none -> 42.5 us  [shift(): return lax.ppermute(a, axis, [(i, (i + k) % n) for i in range(n)])]
    reduce_scatter x1 -> x0, waiting for transfers between devices: 41.7 us -> none  [per_device(): lax.psum_scatter(terms.astype(jnp.bfloat16), 'tp', scatter_dimension=0, t...]
    dynamic_slice x60 -> x1, local copies, waits for them, and re-layouts: 40.2 us -> 0.59 us  [carried(): lax.dynamic_index_in_dim(finals, jnp.maximum(place - 1, 0), 0, False)]
    unnamed x1 -> x0, blocking collectives: 35.1 us -> none
    dot_general x40 -> x7, matrix products: 89.2 us -> 54.1 us  [the longest x1 17.1 us: per_device(): upper = jnp.dot(normed, widening, preferred_element_type=f32)]
    another operation x2 -> x0, loops' own time: 15 us -> none  [the longest x1 15 us: block_pass(): lax.scan(step, (recurrent_state, last_doc, offset), (to_blocks(query_head...]
  transfers between devices with their start and end apart: 6 -> 8, of which waited for: 5 -> 6; matrix products, arithmetic and copies ran while one was open for 5% -> 16% of each run, Pallas kernels for 0% -> 1%
where the time goes in v1:
time: 402 us; the launch traced here: 401 us
  waiting for transfers between devices  263 us (65%)
  matrix products  54.1 us (13%)
  blocking collectives  21.8 us (5%)
  between operations  15.4 us (4%)
  other arithmetic  15.1 us (4%)
  Pallas kernels  13.9 us (3%)
  local copies, waits for them, and re-layouts  11.1 us (3%)
  starting transfers between devices  6.67 us (2%)
    all_gather x1, waiting for transfers between devices, per_device(): shrinking = lax.all_gather(shrinking_projector, 'sp', axis=1, tiled=True)  80.1 us
    all_gather x1, waiting for transfers between devices, per_device(): widening = lax.all_gather(widening_projector, 'sp', axis=0, tiled=True)  78.7 us
    all_gather x1, waiting for transfers between devices, per_device(): switching = lax.all_gather(switching_projector, 'sp', axis=0, tiled=True)  60.1 us
    ppermute x4, waiting for transfers between devices, shift(): return lax.ppermute(a, axis, [(i, (i + k) % n) for i in range(n)])  42.5 us
    all_gather x1, blocking collectives, carried(): smalls = lax.all_gather(small, 'sp').astype(jnp.float32)  21.8 us
    dot_general x1, matrix products, per_device(): upper = jnp.dot(normed, widening, preferred_element_type=f32)  17.1 us
    dot_general x1, matrix products, per_device(): gate = jnp.dot(normed, switching, preferred_element_type=f32)  15.9 us
    pallas_call x1, Pallas kernels, per_device(): pl.pallas_call(local_kernel, out_shape=(jax.ShapeDtypeStruct((rows, heads...  10 us
  transfers between devices with their start and end apart: 8, of which 6 were waited for; matrix products, arithmetic and copies ran while one was open for 16% of the time, Pallas kernels for 1%

profile of v1, /device:TPU:0, one launch (start us, length us, event | category | flops | bytes accessed | tf_op | source)
XLA Modules:
  0.0 401.4 jit_solution(6198820808949198930)
XLA Ops:
  6.5 1.8 broadcast_in_dim.75.doc_ref
  8.3 1.4 reshape.590.docrow_ref
  9.7 1.6 broadcast_in_dim.74.extra_ref
  11.3 10.0 %local_pass.1 = (f32[768,512]{1,0:T(8,128)}, bf16[768,256]{1,0:T(8,128)(2,1)}, bf16[256,128]{1,0:T(8,128)(2,1)}, f32[1,256]{1,0:T(1,128)}) custom-call(bf16[768,256]{1,0:T(8,128)(2,1)} %q_ref.1, bf16[768,256]{1,0:T(8,128)(2,1)} %k_ref.1, bf16[768,512]{1,0:T(8,128)(2,1)} %v_ref.1, bf16[768,256]{1,0:T(8,128)(2,1)} %f_ref.1, f32[1,256]{1,0:T(1,128)} %bitcast.30, ...), custom_call_target="tpu_custom_call" | custom-call | tf_op jit(solution)/shard_map/local_pass/pallas_call | solution.py:179
  23.4 3.1 collective-permute-start.1
  29.4 21.8 %all_gather.21 = bf16[16,6,64]{2,1,0:T(8,128)(2,1)S(1)} all-gather(bf16[1,6,64]{2,1,0:T(8,128)(2,1)S(1)} %maximum_maximum_fusion), channel_id=1, replica_groups=mesh['sp'=16,'tp'=2] {'sp'}, dimensions={0}, use_global_device_ids=true | all-gather | bytes 13056 | tf_op jit(solution)/shard_map/all_gather | solution.py:135
  56.1 1.3 broadcast_select_fusion.11
  57.5 1.3 broadcast_select_fusion.9
  58.8 1.2 broadcast_select_fusion.7
  60.0 1.3 broadcast_select_fusion.5
  61.3 1.3 broadcast_select_fusion.3
  62.5 1.2 broadcast_select_fusion.1
  63.7 1.2 broadcast_select_fusion
  65.0 2.5 fusion.24.state_ref
  67.5 3.9 finish_pass.1
  71.7 3.2 fusion.33
  74.9 16.4 %collective-permute-done = bf16[768,512]{1,0:T(8,128)(2,1)S(1)} collective-permute-done((bf16[768,512]{1,0:T(8,128)(2,1)}, bf16[768,512]{1,0:T(8,128)(2,1)S(1)}, u32[]{:S(2)}, u32[]{:S(2)}) %collective-permute-start) | collective-permute-done | bytes 786464 | tf_op jit(solution)/shard_map/ppermute | solution.py:120
  91.4 3.8 fusion
  95.2 1.7 copy-done
  97.2 60.1 %all-gather.6.cloned.1.call-done = bf16[2048,2816]{1,0:T(8,128)(2,1)} async-done(((bf16[128,2816]{1,0:T(8,128)(2,1)}), bf16[2048,2816]{1,0:T(8,128)(2,1)}) %all-gather.6.cloned.1.call-update) | async-done | bytes 11534352 | tf_op jit(solution)/shard_map/all_gather | solution.py:172
  157.3 15.9 %fusion.9 = f32[768,2816]{1,0:T(8,128)} fusion(bf16[2048,2816]{1,0:T(8,128)(2,1)} %all-gather.6.cloned.1.call-done, bf16[768,2048]{1,0:T(8,128)(2,1)} %copy-done, f32[2048]{0:T(1024)S(1)} %copy-done.5, f32[768]{0:T(1024)S(1)} %add_rsqrt_fusion), kind=kOutput, calls=%fused_computation.19 | convolution fusion | flops 8864661504 | bytes 23342080 | tf_op jit(solution)/shard_map/dot_general | solution.py:216
  173.2 78.7 %all-gather.8.cloned.1.call-done = bf16[2048,2816]{1,0:T(8,128)(2,1)} async-done(((bf16[128,2816]{1,0:T(8,128)(2,1)}), bf16[2048,2816]{1,0:T(8,128)(2,1)}) %all-gather.8.cloned.1.call-update) | async-done | bytes 11534352 | tf_op jit(solution)/shard_map/all_gather | solution.py:173
  251.9 17.1 %multiply_convert_fusion = bf16[768,2816]{1,0:T(8,128)(2,1)} fusion(f32[768,2816]{1,0:T(8,128)} %fusion.9, bf16[2048,2816]{1,0:T(8,128)(2,1)} %all-gather.8.cloned.1.call-done, bf16[768,2048]{1,0:T(8,128)(2,1)} %copy-done, f32[2048]{0:T(1024)S(1)} %copy-done.5, f32[768]{0:T(1024)S(1)} %add_rsqrt_fusion), kind=kOutput, calls=%fused_computation | convolution fusion | flops 8877637632 | bytes 27667456 | tf_op jit(solution)/shard_map/dot_general | solution.py:217
  269.0 80.1 %all-gather.10.cloned.1.call-done = bf16[2816,2048]{1,0:T(8,128)(2,1)} async-done(((bf16[2816,128]{1,0:T(8,128)(2,1)}), bf16[2816,2048]{1,0:T(8,128)(2,1)}) %all-gather.10.cloned.1.call-update) | async-done | bytes 11534352 | tf_op jit(solution)/shard_map/all_gather | solution.py:174
  349.0 7.2 %convolution_convert_fusion.1 = bf16[192,2048]{1,0:T(8,128)(2,1)S(1)} fusion(bf16[2816,2048]{1,0:T(8,128)(2,1)} %all-gather.10.cloned.1.call-done, bf16[768,2816]{1,0:T(8,128)(2,1)} %multiply_convert_fusion, s32[]{:T(128)S(6)} %select_n.674), kind=kOutput, calls=%fused_computation.8 | convolution fusion | flops 2214985728 | bytes 13402116 | tf_op jit(solution)/shard_map/dot_general | solution.py:227
  356.2 1.6 collective-permute-start.3
  358.2 2.4 convolution_convert_fusion.2
  360.6 1.6 collective-permute-start.2
  362.1 4.6 %convolution_convert_fusion = bf16[384,2048]{1,0:T(8,128)(2,1)S(1)} fusion(bf16[2816,2048]{1,0:T(8,128)(2,1)S(1)} %copy-done.4, bf16[768,2816]{1,0:T(8,128)(2,1)S(1)} %copy-done.6, s32[]{:T(128)S(6)} %select_n.671), kind=kOutput, calls=%fused_computation.7 | convolution fusion | flops 4429971456 | bytes 15269892 | tf_op jit(solution)/shard_map/dot_general | solution.py:233
  366.7 9.9 %collective-permute-done.3 = bf16[192,2048]{1,0:T(8,128)(2,1)S(1)} collective-permute-done((bf16[192,2048]{1,0:T(8,128)(2,1)S(1)}, bf16[192,2048]{1,0:T(8,128)(2,1)S(1)}, u32[]{:S(2)}, u32[]{:S(2)}) %collective-permute-start.3) | collective-permute-done | bytes 786464 | tf_op jit(solution)/shard_map/ppermute | solution.py:120
  376.7 16.1 %collective-permute-done.2 = bf16[192,2048]{1,0:T(8,128)(2,1)S(1)} collective-permute-done((bf16[192,2048]{1,0:T(8,128)(2,1)S(1)}, bf16[192,2048]{1,0:T(8,128)(2,1)S(1)}, u32[]{:S(2)}, u32[]{:S(2)}) %collective-permute-start.2) | collective-permute-done | bytes 786464 | tf_op jit(solution)/shard_map/ppermute | solution.py:120
  393.7 1.2 pad_maximum_fusion
  (57 shorter events, 9.8 us)
Async XLA Ops:
  6.5 19.9 %copy-start.3 = (s32[768]{0:T(1024)S(1)}, s32[768]{0:T(1024)}, u32[]{:S(2)}) copy-start(s32[768]{0:T(1024)} %param.23) | copy-start | bytes 9220
  6.5 16.9 %copy-start.2 = (bf16[512,2048]{1,0:T(8,128)(2,1)S(1)}, bf16[512,2048]{1,0:T(8,128)(2,1)}, u32[]{:S(2)}) copy-start(bf16[512,2048]{1,0:T(8,128)(2,1)} %param.25) | copy-start | bytes 6291460
  6.5 58.5 %all-gather.12.cloned.1.call-start = ((), (), s32[]{:S(2)}) async-start(), calls=%async_computation.3 | async-start | bytes 1114112 | tf_op jit(solution)/shard_map/all_gather | solution.py:126
  21.3 136.0 %all-gather.6.cloned.1.call-start = ((), (), s32[]{:S(2)}) async-start(), calls=%async_computation | async-start | bytes 12255232 | tf_op jit(solution)/shard_map/all_gather | solution.py:172
  22.1 229.8 %all-gather.8.cloned.1.call-start = ((), (), s32[]{:S(2)}) async-start(), calls=%async_computation.1 | async-start | bytes 12255232 | tf_op jit(solution)/shard_map/all_gather | solution.py:173
  22.8 326.2 %all-gather.10.cloned.1.call-start = ((), (), s32[]{:S(2)}) async-start(), calls=%async_computation.2 | async-start | bytes 12255232 | tf_op jit(solution)/shard_map/all_gather | solution.py:174
  23.4 51.5 %collective-permute-start.1 = (bf16[512,2048]{1,0:T(8,128)(2,1)S(1)}, bf16[512,2048]{1,0:T(8,128)(2,1)}, u32[]{:S(2)}, u32[]{:S(2)}) collective-permute-start(bf16[512,2048]{1,0:T(8,128)(2,1)S(1)} %copy-done.2), channel_id=1, source_target_pairs={{0,1},{1,0},{2,3},{3,2},{4,5},{5,4},{6,7},{7,6},{8,9},{9,8},{10,11... | collective-permute-start | bytes 6291464 | tf_op jit(solution)/shard_map/ppermute | solution.py:120
  71.4 20.0 %collective-permute-start = (bf16[768,512]{1,0:T(8,128)(2,1)}, bf16[768,512]{1,0:T(8,128)(2,1)S(1)}, u32[]{:S(2)}, u32[]{:S(2)}) collective-permute-start(bf16[768,512]{1,0:T(8,128)(2,1)} %finish_pass.1), channel_id=1, source_target_pairs={{0,1},{1,0},{2,3},{3,2},{4,5},{5,4},{6,7},{7,6},{8,9},{9,8},{10,11... | collective-permute-start | bytes 2359304 | tf_op jit(solution)/shard_map/ppermute | solution.py:120
  71.7 19.6 %copy-start.1 = (bf16[768,2048]{1,0:T(8,128)(2,1)S(1)}, bf16[768,2048]{1,0:T(8,128)(2,1)}, u32[]{:S(2)}) copy-start(bf16[768,2048]{1,0:T(8,128)(2,1)} %param.15) | copy-start | bytes 9437188
  95.2 1.7 copy-start
  95.2 62.1 %copy-start.5 = (f32[2048]{0:T(1024)S(1)}, f32[2048]{0:T(1024)}, u32[]{:S(2)}) copy-start(f32[2048]{0:T(1024)} %param.26) | copy-start | bytes 24580
  349.0 8.7 %copy-start.4 = (bf16[2816,2048]{1,0:T(8,128)(2,1)S(1)}, bf16[2816,2048]{1,0:T(8,128)(2,1)}, u32[]{:S(2)}) copy-start(bf16[2816,2048]{1,0:T(8,128)(2,1)} %all-gather.10.cloned.1.call-done) | copy-start | bytes 34603012
  349.0 9.1 %copy-start.6 = (bf16[768,2816]{1,0:T(8,128)(2,1)S(1)}, bf16[768,2816]{1,0:T(8,128)(2,1)}, u32[]{:S(2)}) copy-start(bf16[768,2816]{1,0:T(8,128)(2,1)} %multiply_convert_fusion) | copy-start | bytes 12976132
  356.2 20.5 %collective-permute-start.3 = (bf16[192,2048]{1,0:T(8,128)(2,1)S(1)}, bf16[192,2048]{1,0:T(8,128)(2,1)S(1)}, u32[]{:S(2)}, u32[]{:S(2)}) collective-permute-start(bf16[192,2048]{1,0:T(8,128)(2,1)S(1)} %convolution_convert_fusion.1), channel_id=1, source_target_pairs={{0,1},{1,0},{2,3},{3,2},{4,5},{5,4},{6,7},{7,6},{8,9},{9,8},{10,11... | collective-permute-start | bytes 2359304 | tf_op jit(solution)/shard_map/ppermute | solution.py:120
  360.6 32.3 %collective-permute-start.2 = (bf16[192,2048]{1,0:T(8,128)(2,1)S(1)}, bf16[192,2048]{1,0:T(8,128)(2,1)S(1)}, u32[]{:S(2)}, u32[]{:S(2)}) collective-permute-start(bf16[192,2048]{1,0:T(8,128)(2,1)S(1)} %convolution_convert_fusion.2), channel_id=1, source_target_pairs={{0,1},{1,0},{2,3},{3,2},{4,5},{5,4},{6,7},{7,6},{8,9},{9,8},{10,11... | collective-permute-start | bytes 2359304 | tf_op jit(solution)/shard_map/ppermute | solution.py:120
Sparse Core Ops, SparseCore 0:
  21.4 40.5 all-gather.11
  64.4 92.8 all-gather.5
  159.6 92.2 all-gather.7
  253.9 95.1 all-gather.9
